TPU v7x, 32 devices: a whole 2x2x4 slice. The times are simulated.
32 devices in a mesh: grp: 2 (over y), fs: 4 (over z), tp: 4 (over x, core).
Axes of the slice: x: 2, y: 2, z: 4, core: 2. Of those that a mesh axis runs over, the one named last changes fastest.
Arguments:
- tokens: bfloat16 [4096, 2048], P(('grp', 'fs')), parts along dimension 0, may hold values from -6 to 6
- pre_gain: float32 [2048], replicated, may hold values from 0.1 to 1.9
- up_weight: float32 [2048, 8192], P('fs', 'tp'), may hold values from -0.125 to 0.125
- up_scale: float32 [8192], P('tp'), may hold values from 0.3 to 3
- down_weight: float32 [8192, 2048], P('tp', 'fs'), may hold values from -0.0625 to 0.0625
- down_scale: float32 [2048], P('fs'), may hold values from 0.3 to 3
- post_gain: float32 [2048], replicated, may hold values from 0.1 to 1.9
Outputs:
- mixed: bfloat16 [4096, 2048], P(('grp', 'fs')), parts along dimension 0
There are 2 independent parts, one for each index of `grp`. A program takes and returns all parts, laid end to end along the dimension named above; an argument that names none is the same for every part. Nothing has to cross between parts.
All inputs are finite; a program needn't handle non-finite values.
Results may differ from a plain program's by a relative error of at most 0.01.
Values may be sent and summed in bfloat16 or wider, within the bound.
A program may use at most 64 MiB of HBM per device.

v0:
```python
import jax
import jax.numpy as jnp
from jax import lax
from jax.sharding import PartitionSpec as P

epsilon = 1e-06


def rms_rows(values, scaling):
    return values * lax.rsqrt(jnp.mean(values * values, axis=-1, keepdims=True) + epsilon) * scaling


def activate(lifted, up_scale):
    return jnp.square(jax.nn.relu(lifted * up_scale)).astype(jnp.bfloat16)


def on_device(tokens, pre_gain, up_weight, up_scale, down_weight, down_scale, post_gain):
    residual = tokens.astype(jnp.float32)
    normed = rms_rows(residual, pre_gain).astype(jnp.bfloat16)
    up_cast = up_weight.astype(jnp.bfloat16)
    down_cast = down_weight.astype(jnp.bfloat16)
    column_scales = lax.all_gather(down_scale, "fs", axis=0, tiled=True)
    up_full, down_full = (
        lax.all_gather(up_cast, "fs", axis=0, tiled=True),
        lax.all_gather(down_cast, "fs", axis=1, tiled=True),
    )
    lifted = jnp.dot(normed, up_full, preferred_element_type=jnp.float32)
    hidden = activate(lifted, up_scale)
    partials = jnp.dot(hidden, down_full, preferred_element_type=jnp.float32)
    partials = (partials * column_scales).astype(jnp.bfloat16)
    summed = lax.psum(partials, "tp").astype(jnp.float32)
    branch = lax.optimization_barrier(summed.astype(jnp.bfloat16)).astype(jnp.float32)
    return (residual + rms_rows(branch, post_gain)).astype(jnp.bfloat16)


def solution(mesh):
    placed = (P(("grp", "fs"), None), P(), P("fs", "tp"), P("tp"), P("tp", "fs"), P("fs"), P())
    return jax.shard_map(
        on_device, mesh=mesh, in_specs=placed, out_specs=P(("grp", "fs"), None), check_vma=False
    )
```

profile of v0, /device:TPU:0, one launch (start us, length us, event | category | flops | bytes accessed | tf_op | source)
XLA Modules:
  0.0 390.7 jit_solution(1393398002839084678)
XLA Ops:
  6.5 0.0 all-gather.4.cloned.1.call-start
  6.5 3.8 convert_element_type.28
  10.4 0.0 all-gather.4.cloned.1.call-update
  10.4 0.0 copy-start.2
  10.4 0.0 copy-start
  10.4 0.0 copy-start.3
  10.4 0.0 copy-start.4
  10.5 0.0 all-gather.6.cloned.1.call-start
  10.5 3.9 %convert_element_type.30 = bf16[2048,512]{1,0:T(8,128)(2,1)} convert(f32[2048,512]{1,0:T(8,128)} %param.11) | non-fusion elementwise | flops 1048576 | bytes 6291456 | tf_op jit(solution)/shard_map/convert_element_type | solution.py:21
  14.4 0.0 all-gather.6.cloned.1.call-update
  14.4 0.0 all-reduce.2.cloned.1.call-start
  14.5 0.0 copy-done.2
  14.5 13.7 %all-gather = f32[4,1,512]{2,1,0:T(1,128)S(1)} all-gather(f32[1,1,512]{2,1,0:T(1,128)S(1)} %bitcast.10), channel_id=1, replica_groups=mesh['grp'=2,'fs'=4,'tp'=4] {'fs'}, dimensions={0}, use_global_device_ids=true | all-gather | bytes 10240 | tf_op jit(solution)/shard_map/all_gather | solution.py:22
  28.2 0.0 copy-done
  28.2 0.5 fusion.2
  28.7 134.2 %all-gather.4.cloned.1.call-done = bf16[2048,2048]{1,0:T(8,128)(2,1)} async-done(((bf16[512,2048]{1,0:T(8,128)(2,1)}), bf16[2048,2048]{1,0:T(8,128)(2,1)}) %all-gather.4.cloned.1.call-update) | async-done | bytes 8388624 | tf_op jit(solution)/shard_map/all_gather | solution.py:24
  162.9 149.4 %all-gather.6.cloned.1.call-done = bf16[2048,2048]{1,0:T(8,128)(2,1)} async-done(((bf16[2048,512]{1,0:T(8,128)(2,1)}), bf16[2048,2048]{1,0:T(8,128)(2,1)}) %all-gather.6.cloned.1.call-update) | async-done | bytes 8388624 | tf_op jit(solution)/shard_map/all_gather | solution.py:25
  312.3 0.0 copy-done.3
  312.3 0.0 copy-done.4
  312.3 16.0 %multiply_convert_fusion = bf16[512,2048]{1,0:T(8,128)(2,1)} fusion(bf16[2048,2048]{1,0:T(8,128)(2,1)} %all-gather.6.cloned.1.call-done, f32[2048]{0:T(1024)S(1)} %bitcast.9, bf16[2048,2048]{1,0:T(8,128)(2,1)} %all-gather.4.cloned.1.call-done, bf16[512,2048]{1,0:T(8,128)(2,1)S(1)} %copy-done, f32[2048]{0:T(1024)S(1)} %copy-done.3, f32[2048]{0:T(1024)S(1)} %copy-done.4, ...), kind=kOutput, calls=%fused_computation.11 | convolution fusion | flops 8600420352 | bytes 20998144 | tf_op jit(solution)/shard_map/dot_general | solution.py:29
  328.3 0.0 copy-start.1
  328.3 0.0 all-reduce.2.cloned.1.call-update
  328.3 49.7 %all-reduce.2.cloned.1.call-done = bf16[512,2048]{1,0:T(8,128)(2,1)} async-done(((bf16[512,2048]{1,0:T(8,128)(2,1)}), bf16[512,2048]{1,0:T(8,128)(2,1)}) %all-reduce.2.cloned.1.call-update) | async-done | bytes 2097168 | tf_op jit(solution)/shard_map/psum | solution.py:31
  378.0 2.1 fusion
  380.1 0.0 copy-done.1
  380.1 4.1 %fusion.5 = bf16[512,2048]{1,0:T(8,128)(2,1)} fusion(bf16[512,2048]{1,0:T(8,128)(2,1)} %all-reduce.2.cloned.1.call-done, bf16[512,2048]{1,0:T(8,128)(2,1)S(1)} %copy-done, f32[2048]{0:T(1024)S(1)} %copy-done.1, f32[512]{0:T(512)S(1)} %add_rsqrt_fusion), kind=kLoop, calls=%fused_computation.10 | loop fusion | flops 6291456 | bytes 6301696 | tf_op jit(solution)/shard_map/convert_element_type | solution.py:33
  (2 shorter events, 0.0 us)
Async XLA Ops:
  6.5 156.4 %all-gather.4.cloned.1.call-start = ((), (), s32[]{:S(2)}) async-start(), calls=%async_computation | async-start | bytes 10485760 | tf_op jit(solution)/shard_map/all_gather | solution.py:24
  10.4 4.1 %copy-start.2 = (f32[512]{0:T(512)S(1)}, f32[512]{0:T(512)}, u32[]{:S(2)}) copy-start(f32[512]{0:T(512)} %param.12) | copy-start | bytes 6148
  10.4 17.8 %copy-start = (bf16[512,2048]{1,0:T(8,128)(2,1)S(1)}, bf16[512,2048]{1,0:T(8,128)(2,1)}, u32[]{:S(2)}) copy-start(bf16[512,2048]{1,0:T(8,128)(2,1)} %param.7) | copy-start | bytes 6291460
  10.4 301.9 %copy-start.3 = (f32[2048]{0:T(1024)S(1)}, f32[2048]{0:T(1024)}, u32[]{:S(2)}) copy-start(f32[2048]{0:T(1024)} %param.10) | copy-start | bytes 24580
  10.4 301.9 %copy-start.4 = (f32[2048]{0:T(1024)S(1)}, f32[2048]{0:T(1024)}, u32[]{:S(2)}) copy-start(f32[2048]{0:T(1024)} %param.8) | copy-start | bytes 24580
  10.5 301.9 %all-gather.6.cloned.1.call-start = ((), (), s32[]{:S(2)}) async-start(), calls=%async_computation.1 | async-start | bytes 10485760 | tf_op jit(solution)/shard_map/all_gather | solution.py:25
  14.4 363.6 %all-reduce.2.cloned.1.call-start = ((), (), s32[]{:S(2)}) async-start(), calls=%async_computation.2 | async-start | bytes 4194304 | tf_op jit(solution)/shard_map/psum | solution.py:31
  328.3 51.8 %copy-start.1 = (f32[2048]{0:T(1024)S(1)}, f32[2048]{0:T(1024)}, u32[]{:S(2)}) copy-start(f32[2048]{0:T(1024)} %param.13) | copy-start | bytes 24580
Sparse Core Ops, SparseCore 0:
  10.5 152.3 all-gather.3
  164.5 147.7 all-gather.5
  328.4 49.5 all-reduce.1
where the time goes:
time: 391 us
  waiting for transfers between devices  333 us (85%)
  matrix products  16 us (4%)
  other arithmetic  14.4 us (4%)
  blocking collectives  13.7 us (4%)
  between operations  13.2 us (3%)
    all_gather x1, waiting for transfers between devices, on_device(): lax.all_gather(down_cast, 'fs', axis=1, tiled=True)  149 us
    all_gather x1, waiting for transfers between devices, on_device(): lax.all_gather(up_cast, 'fs', axis=0, tiled=True)  134 us
    psum x1, waiting for transfers between devices, on_device(): summed = lax.psum(partials, 'tp').astype(jnp.float32)  49.7 us
    dot_general x1, matrix products, on_device(): partials = jnp.dot(hidden, down_full, preferred_element_type=jnp.float32)  16 us
    all_gather x1, blocking collectives, on_device(): column_scales = lax.all_gather(down_scale, 'fs', axis=0, tiled=True)  13.7 us
  transfers between devices with their start and end apart: 3, of which 3 were waited for; matrix products, arithmetic and copies ran while one was open for 1% of the time, Pallas kernels for 0%

commit v1 on v0

--- a/solution.py
+++ b/solution.py
@@ -21,7 +21,12 @@
     down_cast = down_weight.astype(jnp.bfloat16)
     column_scales = lax.all_gather(down_scale, "fs", axis=0, tiled=True)
     up_full, down_full = (
-        lax.all_gather(up_cast, "fs", axis=0, tiled=True),
+        jnp.concatenate(
+            lax.all_to_all(
+                jnp.stack(lax.axis_size("fs") * [up_cast]), "fs", split_axis=0, concat_axis=0
+            ),
+            axis=0,
+        ),
         lax.all_gather(down_cast, "fs", axis=1, tiled=True),
     )
     lifted = jnp.dot(normed, up_full, preferred_element_type=jnp.float32)

time: 391 us -> 424 us (1.084)
  blocking collectives: 13.7 us -> 320 us
  waiting for transfers between devices: 333 us -> 50 us
  starting transfers between devices: 0.09 us -> 6.43 us
  local copies, waits for them, and re-layouts: 0.03 us -> 4.33 us
    all_gather x1, blocking collectives: 13.7 us -> 320 us  [on_device(): column_scales = lax.all_gather(down_scale, 'fs', axis=0, tiled=True)]
    all_gather x1, waiting for transfers between devices: 149 us -> 0.02 us  [on_device(): lax.all_gather(down_cast, 'fs', axis=1, tiled=True)]
    all_gather x1 -> x0, waiting for transfers between devices: 134 us -> none  [on_device(): lax.all_gather(up_cast, 'fs', axis=0, tiled=True)]
    all_to_all x0 -> x1, starting transfers between devices: none -> 6.35 us  [on_device(): lax.all_to_all(jnp.stack(lax.axis_size('fs') * [up_cast]), 'fs', split_ax...]
    another operation x0 -> x1, local copies, waits for them, and re-layouts: none -> 4.31 us  [on_device(): jnp.stack(lax.axis_size('fs') * [up_cast])]
  transfers between devices with their start and end apart: 3 -> 3, of which waited for: 3 -> 1; matrix products, arithmetic and copies ran while one was open for 1% -> 1% of each run, Pallas kernels for 0% -> 0%
where the time goes in v1:
time: 424 us; the launch traced here: 423 us
  blocking collectives  320 us (75%)
  waiting for transfers between devices  50 us (12%)
  matrix products  16 us (4%)
  between operations  13.5 us (3%)
  other arithmetic  13.1 us (3%)
  starting transfers between devices  6.43 us (2%)
  local copies, waits for them, and re-layouts  4.33 us (1%)
    all_gather x1, blocking collectives, on_device(): column_scales = lax.all_gather(down_scale, 'fs', axis=0, tiled=True)  320 us
    psum x1, waiting for transfers between devices, on_device(): summed = lax.psum(partials, 'tp').astype(jnp.float32)  49.9 us
    dot_general x1, matrix products, on_device(): partials = jnp.dot(hidden, down_full, preferred_element_type=jnp.float32)  16 us
  transfers between devices with their start and end apart: 3, of which 1 were waited for; matrix products, arithmetic and copies ran while one was open for 1% of the time, Pallas kernels for 0%

profile of v1, /device:TPU:0, one launch (start us, length us, event | category | flops | bytes accessed | tf_op | source)
XLA Modules:
  0.0 423.3 jit_solution(11032540553369062330)
XLA Ops:
  6.5 2.5 convert_element_type.28
  9.0 4.3 %stack.2 = bf16[4,512,2048]{2,1,0:T(8,128)(2,1)} broadcast(bf16[512,2048]{1,0:T(8,128)(2,1)S(1)} %convert_element_type.28), dimensions={1,2} | broadcast | bytes 10485760 | tf_op jit(solution)/shard_map/stack | solution.py:26
  13.3 6.3 %all-to-all-start = ((bf16[4,512,2048]{2,1,0:T(8,128)(2,1)}), bf16[4,512,2048]{2,1,0:T(8,128)(2,1)}, u32[]{:S(2)}, u32[]{:S(2)}) async-start(bf16[4,512,2048]{2,1,0:T(8,128)(2,1)} %stack.2), calls=%async_computation | async-start | bytes 16777216 | tf_op jit(solution)/shard_map/all_to_all | solution.py:25
  19.7 0.0 copy-start.2
  19.7 0.0 copy-start
  19.7 0.0 copy-start.3
  19.7 0.0 copy-start.4
  19.7 0.0 all-gather.3.cloned.1.call-start
  19.8 3.9 convert_element_type.30
  23.7 0.0 all-gather.3.cloned.1.call-update
  23.7 0.0 all-reduce.2.cloned.1.call-start
  23.8 0.0 copy-done.2
  23.8 320.0 %all-gather = f32[4,1,512]{2,1,0:T(1,128)S(1)} all-gather(f32[1,1,512]{2,1,0:T(1,128)S(1)} %bitcast.11), channel_id=1, replica_groups=mesh['grp'=2,'fs'=4,'tp'=4] {'fs'}, dimensions={0}, use_global_device_ids=true | all-gather | bytes 10240 | tf_op jit(solution)/shard_map/all_gather | solution.py:22
  343.8 0.0 copy-done
  343.8 0.5 fusion.2
  344.3 0.0 all-to-all-done
  344.3 0.0 all-gather.3.cloned.1.call-done
  344.3 0.0 copy-done.3
  344.3 0.0 copy-done.4
  344.3 16.0 %multiply_convert_fusion = bf16[512,2048]{1,0:T(8,128)(2,1)} fusion(bf16[2048,2048]{1,0:T(8,128)(2,1)} %all-gather.3.cloned.1.call-done, f32[2048]{0:T(1024)S(1)} %bitcast.10, bf16[2048,2048]{1,0:T(8,128)(2,1)} %bitcast, bf16[512,2048]{1,0:T(8,128)(2,1)S(1)} %copy-done, f32[2048]{0:T(1024)S(1)} %copy-done.3, f32[2048]{0:T(1024)S(1)} %copy-done.4, ...), kind=kOutput, calls=%fused_computation.11 | convolution fusion | flops 8600420352 | bytes 20998144 | tf_op jit(solution)/shard_map/dot_general | solution.py:34
  360.3 0.0 copy-start.1
  360.3 0.0 all-reduce.2.cloned.1.call-update
  360.3 49.9 %all-reduce.2.cloned.1.call-done = bf16[512,2048]{1,0:T(8,128)(2,1)} async-done(((bf16[512,2048]{1,0:T(8,128)(2,1)}), bf16[512,2048]{1,0:T(8,128)(2,1)}) %all-reduce.2.cloned.1.call-update) | async-done | bytes 2097168 | tf_op jit(solution)/shard_map/psum | solution.py:36
  410.3 2.1 fusion
  412.3 0.0 copy-done.1
  412.3 4.1 fusion.5
  (2 shorter events, 0.0 us)
Async XLA Ops:
  13.3 330.9 %all-to-all-start = ((bf16[4,512,2048]{2,1,0:T(8,128)(2,1)}), bf16[4,512,2048]{2,1,0:T(8,128)(2,1)}, u32[]{:S(2)}, u32[]{:S(2)}) async-start(bf16[4,512,2048]{2,1,0:T(8,128)(2,1)} %stack.2), calls=%async_computation | async-start | bytes 16777216 | tf_op jit(solution)/shard_map/all_to_all | solution.py:25
  19.7 4.1 copy-start.2
  19.7 324.1 %copy-start = (bf16[512,2048]{1,0:T(8,128)(2,1)S(1)}, bf16[512,2048]{1,0:T(8,128)(2,1)}, u32[]{:S(2)}) copy-start(bf16[512,2048]{1,0:T(8,128)(2,1)} %param.7) | copy-start | bytes 6291460
  19.7 324.6 %copy-start.3 = (f32[2048]{0:T(1024)S(1)}, f32[2048]{0:T(1024)}, u32[]{:S(2)}) copy-start(f32[2048]{0:T(1024)} %param.10) | copy-start | bytes 24580
  19.7 324.6 %copy-start.4 = (f32[2048]{0:T(1024)S(1)}, f32[2048]{0:T(1024)}, u32[]{:S(2)}) copy-start(f32[2048]{0:T(1024)} %param.8) | copy-start | bytes 24580
  19.7 324.6 %all-gather.3.cloned.1.call-start = ((), (), s32[]{:S(2)}) async-start(), calls=%async_computation.1 | async-start | bytes 10485760 | tf_op jit(solution)/shard_map/all_gather | solution.py:30
  23.7 386.6 %all-reduce.2.cloned.1.call-start = ((), (), s32[]{:S(2)}) async-start(), calls=%async_computation.2 | async-start | bytes 4194304 | tf_op jit(solution)/shard_map/psum | solution.py:36
  360.3 52.0 %copy-start.1 = (f32[2048]{0:T(1024)S(1)}, f32[2048]{0:T(1024)}, u32[]{:S(2)}) copy-start(f32[2048]{0:T(1024)} %param.13) | copy-start | bytes 24580
Sparse Core Ops, SparseCore 0:
  23.8 293.6 all-gather.2
  360.5 49.7 all-reduce.1
